TPU v7x, 32 devices: a whole 2x2x4 slice. The times are simulated.
32 devices in a mesh: sp: 8 (over z, y), tp: 4 (over x, core).
Axes of the slice: x: 2, y: 2, z: 4, core: 2. Of those that a mesh axis runs over, the one named last changes fastest.
Arguments:
- queries: bfloat16 [1024, 1280], P('sp', 'tp'), may hold values from -4000 to 4000
- latents: bfloat16 [1024, 512], P('sp'), may hold values from -6 to 6
- shared_key: bfloat16 [1024, 64], P('sp'), may hold values from -4 to 4
- expand_weight: bfloat16 [512, 1536], P(None, 'tp'), may hold values from -0.25 to 0.25
- residual: bfloat16 [1024, 2048], P('sp'), may hold values from -3 to 3
- out_weight: bfloat16 [768, 2048], replicated, may hold values from -0.21875 to 0.21875
- norm_gain: bfloat16 [2048], replicated, may hold values from 0.099609375 to 1.8984375
- gate_weight: bfloat16 [2048, 3072], P('sp', 'tp'), may hold values from -0.125 to 0.125
- value_weight: bfloat16 [2048, 3072], P('sp', 'tp'), may hold values from -0.125 to 0.125
- conv_weight: bfloat16 [3, 3072], P(None, 'tp'), may hold values from -3.5 to 3.5
- down_weight: bfloat16 [3072, 2048], P('tp', 'sp'), may hold values from -0.109375 to 0.109375
Outputs:
- output: bfloat16 [1024, 2048], P(('sp', 'tp'))
All inputs are finite; a program needn't handle non-finite values.
Results may differ from a plain program's by a relative error of at most 0.018.
Values may be sent and summed in bfloat16 or wider, within the bound.
A program may use at most 128 MiB of HBM per device.

v0:
```python
import jax
import jax.numpy as jnp
from jax import lax
from jax.sharding import PartitionSpec as P

NOPE_A = 128
VAL_A = 128
NOPE_B = 64
VAL_B = 64
ROPE = 64


def padded_2(block, sides, width):
    for axis, dim in sides:
        count = lax.axis_size(axis)
        forward = [(i, i + 1) for i in range(count - 1)]
        backward = [(target, source) for source, target in forward]
        low = lax.ppermute(
            lax.slice_in_dim(block, block.shape[dim] - width, None, axis=dim), axis, forward
        )
        high = lax.ppermute(lax.slice_in_dim(block, 0, width, axis=dim), axis, backward)
        block = jnp.concatenate([low, block, high], axis=dim)
    return block


def tables(positions, width):
    half_width = width // 2
    frequency = 10000.0 ** (-jnp.arange(half_width, dtype=jnp.float32) / half_width)
    angles = positions.astype(jnp.float32)[:, None] * frequency[None, :]
    return (jnp.cos(angles), jnp.sin(angles))


def rotate(vectors, cos_table, sine_table):
    half_width = vectors.shape[-1] // 2
    first_half = vectors[:, :half_width].astype(jnp.float32)
    second_half = vectors[:, half_width:].astype(jnp.float32)
    turned = jnp.concatenate(
        [
            first_half * cos_table - second_half * sine_table,
            second_half * cos_table + first_half * sine_table,
        ],
        axis=1,
    )
    return turned.astype(jnp.bfloat16)


def normalize(stream, norm_gain):
    stream_f = stream.astype(jnp.float32)
    scaled = stream_f * lax.rsqrt(jnp.mean(stream_f * stream_f, axis=1, keepdims=True) + 1e-06)
    return (scaled * norm_gain.astype(jnp.float32)).astype(jnp.bfloat16)


def update(running, q_content, q_turned, k_content, k_turned, values, score_scale):
    row_max, row_sum, weighted = running
    scores = (
        jnp.einsum("qd,kd->qk", q_content, k_content, preferred_element_type=jnp.float32)
        + jnp.einsum("qd,kd->qk", q_turned, k_turned, preferred_element_type=jnp.float32)
    ) * score_scale
    new_max = jnp.maximum(row_max, jnp.max(scores, axis=1))
    weights = jnp.exp(scores - new_max[:, None])
    row_sum = jnp.sum(weights, axis=1)
    weighted = jnp.dot(weights.astype(jnp.bfloat16), values, preferred_element_type=jnp.float32)
    return (new_max, row_sum, weighted)


def body(
    queries,
    latents,
    shared_key,
    expand_weight,
    residual,
    out_weight,
    norm_gain,
    gate_weight,
    value_weight,
    conv_weight,
    down_weight,
):
    tok_rows = queries.shape[0]
    q_width = NOPE_A + NOPE_B + 2 * ROPE
    kv_width = NOPE_A + VAL_A + NOPE_B + VAL_B
    positions = lax.axis_index("sp") * tok_rows + jnp.arange(tok_rows, dtype=jnp.int32)
    cos_table, sine_table = tables(positions, ROPE)
    key_turned = rotate(shared_key, cos_table, sine_table)
    scale_wide = (NOPE_A + ROPE) ** (-0.5)
    scale_narrow = (NOPE_B + ROPE) ** (-0.5)
    initial = []
    pair_index = 0
    q_base = pair_index * q_width
    rotary_base = q_base + NOPE_A + NOPE_B
    wide_content = queries[:, q_base : q_base + NOPE_A]
    narrow_content = queries[:, q_base + NOPE_A : rotary_base]
    wide_turned = rotate(queries[:, rotary_base : rotary_base + ROPE], cos_table, sine_table)
    narrow_turned = rotate(
        queries[:, rotary_base + ROPE : rotary_base + 2 * ROPE], cos_table, sine_table
    )
    query_parts = [(wide_content, wide_turned, narrow_content, narrow_turned)]
    lowest = jnp.full((tok_rows,), -1e30, jnp.float32)
    empty_sum = jnp.zeros((tok_rows,), jnp.float32)
    initial += [
        lowest,
        empty_sum,
        jnp.zeros((tok_rows, VAL_A), jnp.float32),
        lowest,
        empty_sum,
        jnp.zeros((tok_rows, VAL_B), jnp.float32),
    ]
    initial = tuple(initial)
    pieces = (
        lax.all_gather(latents, "sp", axis=0, tiled=True),
        lax.all_gather(key_turned, "sp", axis=0, tiled=True),
    )
    expanded = jnp.dot(pieces[0], expand_weight, preferred_element_type=jnp.float32).astype(
        jnp.bfloat16
    )
    turned_keys = pieces[1]
    result = []
    pair_index = 0
    wide_content, wide_turned, narrow_content, narrow_turned = query_parts[pair_index]
    kv_base = pair_index * kv_width
    narrow_base = kv_base + NOPE_A + VAL_A
    wide_keys = expanded[:, kv_base : kv_base + NOPE_A]
    wide_values = expanded[:, kv_base + NOPE_A : narrow_base]
    narrow_keys = expanded[:, narrow_base : narrow_base + NOPE_B]
    narrow_values = expanded[:, narrow_base + NOPE_B : narrow_base + NOPE_B + VAL_B]
    absorb_offset = 6 * pair_index
    result += list(
        update(
            initial[absorb_offset : absorb_offset + 3],
            wide_content,
            wide_turned,
            wide_keys,
            turned_keys,
            wide_values,
            scale_wide,
        )
    )
    result += list(
        update(
            initial[absorb_offset + 3 : absorb_offset + 6],
            narrow_content,
            narrow_turned,
            narrow_keys,
            turned_keys,
            narrow_values,
            scale_narrow,
        )
    )
    running = tuple(result)
    outputs = []
    pair_index = 0
    for group_index in range(2):
        offset = 6 * pair_index + 3 * group_index
        outputs.append((running[offset + 2] / running[offset + 1][:, None]).astype(jnp.bfloat16))
    attended = jnp.concatenate(outputs, axis=1)
    share = tok_rows // lax.axis_size("tp")
    tp_index = lax.axis_index("tp")
    all_heads = lax.all_gather(attended, "tp", axis=1, tiled=True)
    projected = jnp.dot(all_heads, out_weight, preferred_element_type=jnp.float32)
    stream = (residual.astype(jnp.float32) + projected).astype(jnp.bfloat16)
    normed = normalize(stream, norm_gain)
    stream_own = lax.dynamic_slice_in_dim(stream, tp_index * share, share, 0)
    pieces = (
        lax.all_gather(gate_weight, "sp", axis=0, tiled=True),
        lax.all_gather(value_weight, "sp", axis=0, tiled=True),
    )
    gate_sum = jnp.dot(normed, pieces[0], preferred_element_type=jnp.float32)
    value_sum = jnp.dot(normed, pieces[1], preferred_element_type=jnp.float32)
    gate_pre = gate_sum.astype(jnp.bfloat16)
    value_pre = value_sum.astype(jnp.bfloat16)
    reach = conv_weight.shape[0] // 2
    padded = padded_2(gate_pre, (("sp", 0),), reach)
    mixed_gate = jnp.zeros(gate_pre.shape, jnp.float32)
    for tap in range(conv_weight.shape[0]):
        mixed_gate = mixed_gate + padded[tap : tap + tok_rows].astype(jnp.float32) * conv_weight[
            tap
        ].astype(jnp.float32)
    active = (jax.nn.silu(mixed_gate) * value_pre.astype(jnp.float32)).astype(jnp.bfloat16)
    partial_rows = jnp.dot(
        active,
        lax.all_gather(down_weight, "sp", axis=1, tiled=True),
        preferred_element_type=jnp.float32,
    )
    summed = lax.psum_scatter(
        partial_rows.astype(jnp.bfloat16), "tp", scatter_dimension=0, tiled=True
    ).astype(jnp.float32)
    return (stream_own.astype(jnp.float32) + summed).astype(jnp.bfloat16)


def solution(mesh):
    in_specs = (
        P("sp", "tp"),
        P("sp", None),
        P("sp", None),
        P(None, "tp"),
        P("sp", None),
        P(),
        P(),
        P("sp", "tp"),
        P("sp", "tp"),
        P(None, "tp"),
        P("tp", "sp"),
    )
    out_specs = P(("sp", "tp"), None)
    return jax.shard_map(body, mesh=mesh, in_specs=in_specs, out_specs=out_specs, check_vma=False)
```

profile of v0, /device:TPU:0, one launch (start us, length us, event | category | flops | bytes accessed | tf_op | source)
XLA Modules:
  0.0 271.1 jit_solution(13108688686888295058)
XLA Ops:
  6.5 0.7 all-gather.5.cloned.1.call-update
  7.3 0.0 all-gather.7.cloned.1.call-start
  7.3 0.7 all-gather.7.cloned.1.call-update
  8.0 0.0 all-gather.11.cloned.1.call-start
  8.1 0.7 all-gather.11.cloned.1.call-update
  8.7 0.0 all-gather.9.cloned.1.call-start
  8.8 0.5 all-gather.9.cloned.1.call-update
  9.3 0.0 reduce-scatter.2.cloned.1.call-start
  9.4 0.7 convert_element_type.113
  10.1 0.9 fusion.59
  11.0 28.2 %all_gather.19 = bf16[1024,64]{0,1:T(8,128)(2,1)S(1)} all-gather(bf16[128,64]{0,1:T(8,128)(2,1)S(1)} %pad_maximum_fusion.5), channel_id=1, replica_groups=mesh['sp'=8,'tp'=4] {'sp'}, dimensions={0}, use_global_device_ids=true | all-gather | bytes 147456 | tf_op jit(solution)/shard_map/all_gather | solution.py:111
  39.2 13.5 %all-gather.5.cloned.1.call-done = bf16[1024,512]{1,0:T(8,128)(2,1)} async-done(((bf16[128,512]{1,0:T(8,128)(2,1)}), bf16[1024,512]{1,0:T(8,128)(2,1)}) %all-gather.5.cloned.1.call-update) | async-done | bytes 1048592 | tf_op jit(solution)/shard_map/all_gather | solution.py:110
  52.7 1.9 convolution_convert_fusion.1
  54.7 0.3 convolution_bitcast_fusion.1
  54.9 0.4 fusion.83
  55.3 0.2 fusion.11
  55.5 0.3 convolution_bitcast_fusion
  55.7 0.4 fusion.82
  56.1 0.2 fusion.13
  56.3 0.2 fusion.7
  56.5 0.3 fusion.6
  56.8 5.6 %all_gather.20 = bf16[128,768]{0,1:T(8,128)(2,1)S(1)} all-gather(bf16[128,192]{0,1:T(8,128)(2,1)S(1)} %pad_maximum_fusion.4), channel_id=1, replica_groups=mesh['sp'=8,'tp'=4] {'tp'}, dimensions={1}, use_global_device_ids=true | all-gather | bytes 245760 | tf_op jit(solution)/shard_map/all_gather | solution.py:158
  62.4 1.4 fusion.8
  63.8 49.9 %all-gather.7.cloned.1.call-done = bf16[2048,768]{1,0:T(8,128)(2,1)} async-done(((bf16[256,768]{1,0:T(8,128)(2,1)}), bf16[2048,768]{1,0:T(8,128)(2,1)}) %all-gather.7.cloned.1.call-update) | async-done | bytes 3145744 | tf_op jit(solution)/shard_map/all_gather | solution.py:164
  113.7 2.7 convolution_convert_fusion.3
  116.4 2.5 collective-permute-start
  118.8 1.3 collective-permute-start.1
  120.2 56.9 %all-gather.11.cloned.1.call-done = bf16[768,2048]{1,0:T(8,128)(2,1)} async-done(((bf16[768,256]{1,0:T(8,128)(2,1)}), bf16[768,2048]{1,0:T(8,128)(2,1)}) %all-gather.11.cloned.1.call-update) | async-done | bytes 3145744 | tf_op jit(solution)/shard_map/all_gather | solution.py:181
  177.1 60.3 %all-gather.9.cloned.1.call-done = bf16[2048,768]{1,0:T(8,128)(2,1)} async-done(((bf16[256,768]{1,0:T(8,128)(2,1)}), bf16[2048,768]{1,0:T(8,128)(2,1)}) %all-gather.9.cloned.1.call-update) | async-done | bytes 3145744 | tf_op jit(solution)/shard_map/all_gather | solution.py:165
  237.3 5.1 %convolution_convert_fusion = bf16[128,2048]{1,0:T(8,128)(2,1)} fusion(bf16[768,2048]{1,0:T(8,128)(2,1)} %all-gather.11.cloned.1.call-done, bf16[2048,768]{1,0:T(8,128)(2,1)} %all-gather.9.cloned.1.call-done, bf16[128,768]{1,0:T(8,128)(2,1)S(1)} %convolution_convert_fusion.3, bf16[1,768]{1,0:T(2,128)(2,1)S(1)} %collective-permute-done.1, ...), kind=kOutput, calls=%fused_computation.2 | convolution fusion | flops 808779776 | bytes 7557632 | tf_op jit(solution)/shard_map/dot_general | solution.py:179
  242.5 20.5 %reduce-scatter.2.cloned.1.call-done = bf16[32,2048]{1,0:T(8,128)(2,1)} async-done(((bf16[128,2048]{1,0:T(8,128)(2,1)}), bf16[32,2048]{1,0:T(8,128)(2,1)}) %reduce-scatter.2.cloned.1.call-update) | async-done | bytes 131088 | tf_op jit(solution)/shard_map/reduce_scatter | solution.py:184
  262.9 1.7 add_convert_fusion
  (21 shorter events, 0.1 us)
Async XLA Ops:
  6.5 55.8 %copy-start = (bf16[768,2048]{1,0:T(8,128)(2,1)S(1)}, bf16[768,2048]{1,0:T(8,128)(2,1)}, u32[]{:S(2)}) copy-start(bf16[768,2048]{1,0:T(8,128)(2,1)} %param.16) | copy-start | bytes 9437188
  6.5 48.1 %copy-start.2 = (bf16[128,320]{0,1:T(8,128)(2,1)S(1)}, bf16[128,320]{0,1:T(8,128)(2,1)}, u32[]{:S(2)}) copy-start(bf16[128,320]{0,1:T(8,128)(2,1)} %param.11) | copy-start | bytes 245764
  6.5 46.2 %all-gather.5.cloned.1.call-start = ((), (), s32[]{:S(2)}) async-start(), calls=%async_computation.1 | async-start | bytes 1179648 | tf_op jit(solution)/shard_map/all_gather | solution.py:110
  7.3 106.4 %all-gather.7.cloned.1.call-start = ((), (), s32[]{:S(2)}) async-start(), calls=%async_computation.2 | async-start | bytes 3538944 | tf_op jit(solution)/shard_map/all_gather | solution.py:164
  8.0 169.1 %all-gather.11.cloned.1.call-start = ((), (), s32[]{:S(2)}) async-start(), calls=%async_computation.4 | async-start | bytes 3538944 | tf_op jit(solution)/shard_map/all_gather | solution.py:181
  8.7 228.6 %all-gather.9.cloned.1.call-start = ((), (), s32[]{:S(2)}) async-start(), calls=%async_computation.3 | async-start | bytes 3538944 | tf_op jit(solution)/shard_map/all_gather | solution.py:165
  9.3 253.6 %reduce-scatter.2.cloned.1.call-start = ((), (), s32[]{:S(2)}) async-start(), calls=%async_computation.5 | async-start | bytes 655360 | tf_op jit(solution)/shard_map/reduce_scatter | solution.py:184
  54.9 7.4 %copy-start.1 = (bf16[128,2048]{1,0:T(8,128)(2,1)S(1)}, bf16[128,2048]{1,0:T(8,128)(2,1)}, u32[]{:S(2)}) copy-start(bf16[128,2048]{1,0:T(8,128)(2,1)} %param.15) | copy-start | bytes 1572868
  62.4 57.8 %copy-start.3 = (bf16[3,768]{1,0:T(4,128)(2,1)S(1)}, bf16[3,768]{1,0:T(4,128)(2,1)}, u32[]{:S(2)}) copy-start(bf16[3,768]{1,0:T(4,128)(2,1)} %param.20) | copy-start | bytes 13828
  116.4 121.0 %collective-permute-start = (bf16[1,768]{1,0:T(2,128)(2,1)S(1)}, bf16[1,768]{1,0:T(2,128)(2,1)S(1)}, u32[]{:S(2)}, u32[]{:S(2)}) collective-permute-start(bf16[1,768]{1,0:T(2,128)(2,1)S(1)} %get-tuple-element.8), channel_id=1, source_target_pairs={{0,4},{4,8},{8,12},{12,16},{16,20},{20,24},{24,28},{1,5},{5,9},{9,... | collective-permute-start | bytes 4616 | tf_op jit(solution)/shard_map/ppermute | solution.py:18
  118.8 118.5 %collective-permute-start.1 = (bf16[1,768]{1,0:T(2,128)(2,1)S(1)}, bf16[1,768]{1,0:T(2,128)(2,1)S(1)}, u32[]{:S(2)}, u32[]{:S(2)}) collective-permute-start(bf16[1,768]{1,0:T(2,128)(2,1)S(1)} %get-tuple-element.9), channel_id=1, source_target_pairs={{4,0},{8,4},{12,8},{16,12},{20,16},{24,20},{28,24},{5,1},{9,5},{13... | collective-permute-start | bytes 4616 | tf_op jit(solution)/shard_map/ppermute | solution.py:21
Sparse Core Ops, SparseCore 0:
  9.5 43.2 all-gather.4
  54.9 58.7 all-gather.6
  115.7 61.2 all-gather.10
  179.1 58.1 all-gather.8
  242.6 20.2 reduce-scatter.1
where the time goes:
time: 271 us
  waiting for transfers between devices  204 us (75%)
  blocking collectives  33.8 us (12%)
  between operations  13.3 us (5%)
  matrix products  12.8 us (5%)
  starting transfers between devices  3.9 us (1%)
  other arithmetic  3.68 us (1%)
    all_gather x1, waiting for transfers between devices, body(): lax.all_gather(value_weight, 'sp', axis=0, tiled=True)  60.3 us
    all_gather x1, waiting for transfers between devices, body(): lax.all_gather(down_weight, 'sp', axis=1, tiled=True)  56.9 us
    all_gather x1, waiting for transfers between devices, body(): lax.all_gather(gate_weight, 'sp', axis=0, tiled=True)  49.9 us
    all_gather x1, blocking collectives, body(): lax.all_gather(key_turned, 'sp', axis=0, tiled=True)  28.2 us
    reduce_scatter x1, waiting for transfers between devices, body(): lax.psum_scatter(partial_rows.astype(jnp.bfloat16), 'tp', scatter_dimensi...  20.5 us
    all_gather x1, waiting for transfers between devices, body(): lax.all_gather(latents, 'sp', axis=0, tiled=True)  13.5 us
    all_gather x1, blocking collectives, body(): all_heads = lax.all_gather(attended, 'tp', axis=1, tiled=True)  5.6 us
  transfers between devices with their start and end apart: 7, of which 5 were waited for; matrix products, arithmetic and copies ran while one was open for 4% of the time, Pallas kernels for 0%

commit v1 on v0

--- a/solution.py
+++ b/solution.py
@@ -1,6 +1,10 @@
+import functools
+
 import jax
 import jax.numpy as jnp
 from jax import lax
+from jax.experimental import pallas as pl
+from jax.experimental.pallas import tpu as pltpu
 from jax.sharding import PartitionSpec as P
 
 NOPE_A = 128
@@ -187,6 +191,353 @@
     return (stream_own.astype(jnp.float32) + summed).astype(jnp.bfloat16)
 
 
+MESH = pl.DeviceIdType.MESH
+
+
+def layer_kernel(
+    zn,
+    table_ref,
+    q_ref,
+    lat_ref,
+    key_ref,
+    expand_ref,
+    res_ref,
+    out_w_ref,
+    gain_ref,
+    gate_ref,
+    value_ref,
+    conv_ref,
+    down_ref,
+    out_ref,
+    lat_all,
+    att_send,
+    att_recv,
+    nrm,
+    stage,
+    w_full,
+    dn_full,
+    hbuf,
+    abuf,
+    halo_send,
+    halo_recv,
+    part,
+    c_send,
+    c_recv,
+    keep,
+    x_send,
+    x_recv,
+    z_send,
+    z_recv,
+    lz_s, lz_r, ly_s, ly_r, lc_s, lc_r,
+    wz_s, wz_r, wy_s, wy_r,
+    dz_s, dz_r, dy_s, dy_r,
+    at_s, at_r,
+    nz_s, nz_r, nx_s, nx_r, nc_s, nc_r,
+    h_s, h_r,
+    pc_s, pc_r, px_s, px_r, pz_s, pz_r,
+):
+    f32, bf16 = jnp.float32, jnp.bfloat16
+    s, t = lax.axis_index("sp"), lax.axis_index("tp")
+    z, y = s // 2, s % 2
+    x, c = t // 2, t % 2
+    yo, xo, co = 1 - y, 1 - x, 1 - c
+    rows = q_ref.shape[0]
+    half, share = rows // 2, rows // 4
+    rank = lat_ref.shape[1]
+    sub = down_ref.shape[0] // zn
+    sp = 2 * zn
+
+    def to_z(d):
+        return {"sp": 2 * ((z + d) % zn) + y, "tp": t}
+
+    y_dev = {"sp": 2 * z + yo, "tp": t}
+    x_dev = {"sp": s, "tp": 2 * xo + c}
+    c_dev = {"sp": s, "tp": 2 * x + co}
+
+    def from_z(d):
+        return (z + zn - d) % zn
+
+    started = []
+
+    def send(src, dst, s_sem, r_sem, dev):
+        copy = pltpu.make_async_remote_copy(
+            src_ref=src, dst_ref=dst, send_sem=s_sem, recv_sem=r_sem,
+            device_id=dev, device_id_type=MESH,
+        )
+        copy.start()
+        started.append(copy)
+        return copy
+
+    def arrived(dst, s_sem, r_sem):
+        pltpu.make_async_remote_copy(
+            src_ref=dst, dst_ref=dst, send_sem=s_sem, recv_sem=r_sem,
+            device_id=c_dev, device_id_type=MESH,
+        ).wait_recv()
+
+    barrier = pltpu.get_barrier_semaphore()
+    partners = [to_z(d) for d in range(1, zn)] + [y_dev, x_dev, c_dev, {"sp": s, "tp": 2 * xo + co}]
+    for dev in partners:
+        pl.semaphore_signal(barrier, inc=1, device_id=dev, device_id_type=MESH)
+
+    cos2 = table_ref[:, : 2 * (ROPE // 2)]
+    sin2 = table_ref[:, ROPE : 2 * ROPE]
+
+    def turn(v):
+        v = v.astype(f32)
+        h = ROPE // 2
+        swapped = jnp.concatenate([v[:, h:], v[:, :h]], axis=1)
+        return (v * cos2 + swapped * sin2).astype(bf16)
+
+    key_turned = turn(key_ref[...])
+    for i in range(2):
+        lat_all[s, i, :, :rank] = lat_ref[i * half : (i + 1) * half, :]
+        lat_all[s, i, :, rank : rank + ROPE] = key_turned[i * half : (i + 1) * half, :]
+        lat_all[s, i, :, rank + ROPE :] = jnp.zeros((half, ROPE), bf16)
+    pl.semaphore_wait(barrier, len(partners))
+
+    mine = lat_all.at[s, c]
+    for d in range(1, zn):
+        send(mine, mine, lz_s.at[d], lz_r.at[d], to_z(d))
+    send(mine, mine, ly_s.at[0], ly_r.at[0], y_dev)
+
+    for k in range(zn):
+        stage[k, :, :sub] = gate_ref[:, k * sub : (k + 1) * sub]
+        stage[k, :, sub:] = value_ref[:, k * sub : (k + 1) * sub]
+
+    for d in range(1, zn):
+        blk = lat_all.at[2 * from_z(d) + y, c]
+        arrived(blk, lz_s.at[d], lz_r.at[d])
+        send(blk, blk, ly_s.at[d], ly_r.at[d], y_dev)
+        send(blk, blk, lc_s.at[d], lc_r.at[d], c_dev)
+    w_full[s] = stage[z]
+    dn_full[s] = down_ref[pl.ds(pl.multiple_of(z * sub, sub), sub), :]
+    for d in range(1, zn):
+        zz = (z + d) % zn
+        send(stage.at[zz], w_full.at[s], wz_s.at[d], wz_r.at[d], to_z(d))
+        send(down_ref.at[pl.ds(pl.multiple_of(zz * sub, sub), sub), :], dn_full.at[s], dz_s.at[d], dz_r.at[d], to_z(d))
+    for d in range(zn):
+        blk = lat_all.at[2 * from_z(d) + yo, c]
+        arrived(blk, ly_s.at[d], ly_r.at[d])
+        send(blk, blk, lc_s.at[zn + d], lc_r.at[zn + d], c_dev)
+    send(w_full.at[s], w_full.at[s], wy_s.at[0], wy_r.at[0], y_dev)
+    send(dn_full.at[s], dn_full.at[s], dy_s.at[0], dy_r.at[0], y_dev)
+    q_wide = q_ref[:, :NOPE_A]
+    q_narrow = q_ref[:, NOPE_A : NOPE_A + NOPE_B]
+    rot = NOPE_A + NOPE_B
+    q_wide_t = turn(q_ref[:, rot : rot + ROPE])
+    q_narrow_t = turn(q_ref[:, rot + ROPE : rot + 2 * ROPE])
+    for d in range(1, zn):
+        arrived(lat_all.at[2 * from_z(d) + y, co], lc_s.at[d], lc_r.at[d])
+    for d in range(zn):
+        arrived(lat_all.at[2 * from_z(d) + yo, co], lc_s.at[zn + d], lc_r.at[zn + d])
+
+    whole = lat_all[...].reshape(sp * rows, lat_all.shape[3])
+    expanded = jnp.dot(whole[:, :rank], expand_ref[...], preferred_element_type=f32).astype(bf16)
+    keys_t = whole[:, rank : rank + ROPE]
+
+    def attend(qc, qt, kc, v, scale):
+        dims = (((1,), (1,)), ((), ()))
+        scores = (
+            lax.dot_general(qc, kc, dims, preferred_element_type=f32)
+            + lax.dot_general(qt, keys_t, dims, preferred_element_type=f32)
+        ) * scale
+        w = jnp.exp(scores - jnp.max(scores, axis=1, keepdims=True))
+        total = jnp.sum(w, axis=1, keepdims=True)
+        return (jnp.dot(w.astype(bf16), v, preferred_element_type=f32) / total).astype(bf16)
+
+    nb = NOPE_A + VAL_A
+    wide = attend(q_wide, q_wide_t, expanded[:, :NOPE_A], expanded[:, NOPE_A:nb], (NOPE_A + ROPE) ** -0.5)
+    narrow = attend(
+        q_narrow, q_narrow_t, expanded[:, nb : nb + NOPE_B],
+        expanded[:, nb + NOPE_B : nb + NOPE_B + VAL_B], (NOPE_B + ROPE) ** -0.5,
+    )
+    vals = VAL_A + VAL_B
+    for i in range(4):
+        att_send[i, :, :VAL_A] = wide[i * share : (i + 1) * share, :]
+        att_send[i, :, VAL_A:vals] = narrow[i * share : (i + 1) * share, :]
+    others = [(2 * x + co), (2 * xo + c), (2 * xo + co)]
+    for i, o in enumerate(others):
+        send(att_send.at[o], att_recv.at[t], at_s.at[i], at_r.at[i], {"sp": s, "tp": o})
+    att_recv[t] = att_send[t]
+
+    def forward_weights(d):
+        blk = w_full.at[2 * from_z(d) + y]
+        arrived(blk, wz_s.at[d], wz_r.at[d])
+        send(blk, blk, wy_s.at[d], wy_r.at[d], y_dev)
+        blk = dn_full.at[2 * from_z(d) + y]
+        arrived(blk, dz_s.at[d], dz_r.at[d])
+        send(blk, blk, dy_s.at[d], dy_r.at[d], y_dev)
+
+    for i, o in enumerate(others):
+        arrived(att_recv.at[o], at_s.at[i], at_r.at[i])
+    projected = jnp.dot(att_recv[0, :, :vals], out_w_ref[:vals, :], preferred_element_type=f32)
+    for i in range(1, 4):
+        projected += jnp.dot(
+            att_recv[i, :, :vals], out_w_ref[i * vals : (i + 1) * vals, :], preferred_element_type=f32
+        )
+    mine_rows = pl.ds(pl.multiple_of(t * share, share), share)
+    stream = (res_ref[mine_rows, :].astype(f32) + projected).astype(bf16)
+    stream_f = stream.astype(f32)
+    scaled = stream_f * lax.rsqrt(jnp.mean(stream_f * stream_f, axis=1, keepdims=True) + 1e-06)
+    nrm[z, t] = (scaled * gain_ref[...].astype(f32)).astype(bf16)
+
+    own = nrm.at[z, t]
+    for d in range(1, zn):
+        send(own, own, nz_s.at[d], nz_r.at[d], to_z(d))
+    send(own, own, nx_s.at[0], nx_r.at[0], x_dev)
+    send(own, own, nc_s.at[0], nc_r.at[0], c_dev)
+    forward_weights(1)
+    xt = 2 * xo + c
+    blk = nrm.at[z, xt]
+    arrived(blk, nx_s.at[0], nx_r.at[0])
+    send(blk, blk, nc_s.at[zn], nc_r.at[zn], c_dev)
+    for d in range(1, zn):
+        blk = nrm.at[from_z(d), t]
+        arrived(blk, nz_s.at[d], nz_r.at[d])
+        send(blk, blk, nx_s.at[d], nx_r.at[d], x_dev)
+        send(blk, blk, nc_s.at[d], nc_r.at[d], c_dev)
+        if d > 1:
+            forward_weights(d)
+    for d in range(1, zn):
+        blk = nrm.at[from_z(d), xt]
+        arrived(blk, nx_s.at[d], nx_r.at[d])
+        send(blk, blk, nc_s.at[zn + d], nc_r.at[zn + d], c_dev)
+    for d in range(zn):
+        arrived(w_full.at[2 * from_z(d) + yo], wy_s.at[d], wy_r.at[d])
+    weights = w_full[...].reshape(sp * w_full.shape[1], 2 * sub)
+    for d in range(zn):
+        zz = from_z(d)
+        arrived(nrm.at[zz, 2 * x + co], nc_s.at[d], nc_r.at[d])
+        arrived(nrm.at[zz, 2 * xo + co], nc_s.at[zn + d], nc_r.at[zn + d])
+        block = nrm[zz].reshape(rows, nrm.shape[3])
+        hbuf[zz] = jnp.dot(block, weights, preferred_element_type=f32).astype(bf16)
+
+    wide_lanes = halo_send.shape[1]
+    for k in range(zn):
+        g = hbuf[k, :, :wide_lanes].astype(f32)
+        halo_send[k : k + 1, :] = g[rows - 1 : rows, :]
+        halo_send[zn + k : zn + k + 1, :] = g[0:1, :]
+    send(halo_send, halo_recv, h_s.at[0], h_r.at[0], y_dev)
+    taps = jnp.zeros((conv_ref.shape[0], wide_lanes), f32)
+    conv_all = conv_ref[...].astype(f32)
+    pieces = [conv_all[:, k * sub : (k + 1) * sub] for k in range(zn)]
+    taps = pieces[0]
+    for k in range(1, zn):
+        taps = jnp.where(z == k, pieces[k], taps)
+    taps = jnp.concatenate([taps, jnp.zeros((taps.shape[0], wide_lanes - sub), f32)], axis=1)
+    row_id = lax.broadcasted_iota(jnp.int32, (rows, wide_lanes), 0)
+    arrived(halo_recv, h_s.at[0], h_r.at[0])
+    nothing = jnp.zeros((1, wide_lanes), f32)
+    for k in range(zn):
+        before_low = halo_recv[k - 1 : k, :] if k > 0 else nothing
+        before = jnp.where(y == 0, before_low, halo_recv[k : k + 1, :])
+        after_high = halo_recv[zn + k + 1 : zn + k + 2, :] if k < zn - 1 else nothing
+        after = jnp.where(y == 0, halo_recv[zn + k : zn + k + 1, :], after_high)
+        g = hbuf[k, :, :wide_lanes].astype(f32)
+        up = jnp.where(row_id == 0, before, pltpu.roll(g, 1, 0))
+        down = jnp.where(row_id == rows - 1, after, pltpu.roll(g, rows - 1, 0))
+        mixed = up * taps[0:1] + g * taps[1:2] + down * taps[2:3]
+        mixed = mixed[:, :sub]
+        v = hbuf[k].astype(f32)[:, sub:]
+        abuf[k] = (mixed / (1.0 + jnp.exp(-mixed)) * v).astype(bf16)
+
+    for d in range(zn):
+        arrived(dn_full.at[2 * from_z(d) + yo], dy_s.at[d], dy_r.at[d])
+    order = list(range(1, zn)) + [0]
+    depth = dn_full.shape[2]
+    for d in order:
+        zz = (z + d) % zn
+        a = abuf[zz]
+        for k in range(sp):
+            p = jnp.dot(a, dn_full[k], preferred_element_type=f32)
+            part[d, :, :, k * depth : (k + 1) * depth] = p.reshape(4, share, depth)
+        for i in range(2):
+            c_send[d, i] = part[d, 2 * i + co].astype(bf16)
+        send(c_send.at[d], c_recv.at[d], pc_s.at[d], pc_r.at[d], c_dev)
+    for d in order:
+        arrived(c_recv.at[d], pc_s.at[d], pc_r.at[d])
+        x_send[d] = (part[d, 2 * xo + c] + c_recv[d, xo].astype(f32)).astype(bf16)
+        send(x_send.at[d], x_recv.at[d], px_s.at[d], px_r.at[d], x_dev)
+        keep[d] = part[d, 2 * x + c] + c_recv[d, x].astype(f32)
+    for d in order:
+        arrived(x_recv.at[d], px_s.at[d], px_r.at[d])
+        if d > 0:
+            z_send[d] = (keep[d] + x_recv[d].astype(f32)).astype(bf16)
+            send(z_send.at[d], z_recv.at[d], pz_s.at[d], pz_r.at[d], to_z(d))
+    total = keep[0] + x_recv[0].astype(f32)
+    for d in range(1, zn):
+        arrived(z_recv.at[d], pz_s.at[d], pz_r.at[d])
+        total += z_recv[d].astype(f32)
+    out_ref[...] = (stream_f + total).astype(bf16)
+    for copy in started:
+        copy.wait_send()
+
+
+def kernel_body(zn, *args):
+    (queries, latents, shared_key, expand_weight, residual, out_weight, norm_gain,
+     gate_weight, value_weight, conv_weight, down_weight) = args
+    rows, width = residual.shape
+    sub = down_weight.shape[0] // zn
+    share, half = rows // 4, rows // 2
+    d_own = gate_weight.shape[0]
+    positions = lax.axis_index("sp") * rows + jnp.arange(rows, dtype=jnp.int32)
+    cos_table, sine_table = tables(positions, ROPE)
+    table = jnp.concatenate([cos_table, cos_table, -sine_table, sine_table], axis=1)
+    bf16, f32 = jnp.bfloat16, jnp.float32
+    vals = VAL_A + VAL_B
+    lanes = -(-vals // 128) * 128
+    halo_lanes = -(-sub // 128) * 128
+    V, DMA = pltpu.VMEM, pltpu.SemaphoreType.DMA
+    sems = []
+    for count in (zn, zn, 2 * zn, zn, zn, zn, zn, 3, zn, zn, 2 * zn, 1, zn, zn, zn):
+        sems += [DMA((count,)), DMA((count,))]
+    return pl.pallas_call(
+        functools.partial(layer_kernel, zn),
+        out_shape=jax.ShapeDtypeStruct((share, width), bf16),
+        in_specs=[pl.BlockSpec(memory_space=V)] * 12,
+        out_specs=pl.BlockSpec(memory_space=V),
+        scratch_shapes=[
+            V((2 * zn, 2, half, latents.shape[1] + 2 * ROPE), bf16),
+            V((4, share, lanes), bf16),
+            V((4, share, lanes), bf16),
+            V((zn, 4, share, width), bf16),
+            V((zn, d_own, 2 * sub), bf16),
+            V((2 * zn, d_own, 2 * sub), bf16),
+            V((2 * zn, sub, down_weight.shape[1]), bf16),
+            V((zn, rows, 2 * sub), bf16),
+            V((zn, rows, sub), bf16),
+            V((2 * zn, halo_lanes), f32),
+            V((2 * zn, halo_lanes), f32),
+            V((zn, 4, share, width), f32),
+            V((zn, 2, share, width), bf16),
+            V((zn, 2, share, width), bf16),
+            V((zn, share, width), f32),
+            V((zn, share, width), bf16),
+            V((zn, share, width), bf16),
+            V((zn, share, width), bf16),
+            V((zn, share, width), bf16),
+        ] + sems,
+        compiler_params=pltpu.CompilerParams(collective_id=0, has_side_effects=True),
+    )(table, queries, latents, shared_key, expand_weight, residual, out_weight,
+      norm_gain.reshape(1, -1), gate_weight, value_weight, conv_weight, down_weight)
+
+
+def pick(*args):
+    zn = lax.axis_size("sp") // 2
+    hidden = args[10].shape[0]
+    sub = hidden // zn
+    fits = (
+        lax.axis_size("sp") % 2 == 0
+        and lax.axis_size("tp") == 4
+        and hidden % zn == 0
+        and sub % 64 == 0
+        and args[7].shape[0] % 128 == 0
+        and args[0].shape[0] % 64 == 0
+        and args[9].shape[0] == 3
+    )
+    return kernel_body(zn, *args) if fits else body(*args)
+
+
 def solution(mesh):
     in_specs = (
         P("sp", "tp"),
@@ -202,4 +553,4 @@
         P("tp", "sp"),
     )
     out_specs = P(("sp", "tp"), None)
-    return jax.shard_map(body, mesh=mesh, in_specs=in_specs, out_specs=out_specs, check_vma=False)
+    return jax.shard_map(pick, mesh=mesh, in_specs=in_specs, out_specs=out_specs, check_vma=False)

time: 271 us -> 97.2 us (0.36)
  waiting for transfers between devices: 204 us -> 0 us
  Pallas kernels: 0 us -> 89.1 us
  blocking collectives: 33.8 us -> 0 us
  between operations: 13.3 us -> 0.02 us
  matrix products: 12.8 us -> 0 us
  local copies, waits for them, and re-layouts: 0.03 us -> 5.91 us
  starting transfers between devices: 3.9 us -> 0 us
    all_gather x4 -> x0, waiting for transfers between devices: 181 us -> none  [the longest x1 60.3 us: body(): lax.all_gather(value_weight, 'sp', axis=0, tiled=True)]
    pallas_call x0 -> x1, Pallas kernels: none -> 89.1 us  [kernel_body(): pl.pallas_call(functools.partial(layer_kernel, zn), out_shape=jax.ShapeDt...]
    all_gather x2 -> x0, blocking collectives: 33.8 us -> none  [the longest x1 28.2 us: body(): lax.all_gather(key_turned, 'sp', axis=0, tiled=True)]
    reduce_scatter x1 -> x0, waiting for transfers between devices: 20.5 us -> none  [body(): lax.psum_scatter(partial_rows.astype(jnp.bfloat16), 'tp', scatter_dimensi...]
    dot_general x10 -> x0, matrix products: 12.8 us -> none  [the longest x1 5.1 us: body(): jnp.dot(active, lax.all_gather(down_weight, 'sp', axis=1, tiled=True), pr...]
    unnamed x8 -> x3, local copies, waits for them, and re-layouts: 0.02 us -> 4.63 us
    ppermute x2 -> x0, starting transfers between devices: 3.75 us -> none  [the longest x1 2.45 us: padded_2(): lax.ppermute(lax.slice_in_dim(block, block.shape[dim] - width, None, axis...]
  transfers between devices with their start and end apart: 7 -> 0, of which waited for: 5 -> 0; matrix products, arithmetic and copies ran while one was open for 4% -> 0% of each run, Pallas kernels for 0% -> 0%
where the time goes in v1:
time: 97.2 us; the launch traced here: 96.1 us
  Pallas kernels  89.1 us (92%)
  local copies, waits for them, and re-layouts  5.91 us (6%)
  other arithmetic  1.08 us (1%)
    pallas_call x1, Pallas kernels, kernel_body(): pl.pallas_call(functools.partial(layer_kernel, zn), out_shape=jax.ShapeDt...  89.1 us
    unnamed x3, local copies, waits for them, and re-layouts  4.63 us

profile of v1, /device:TPU:0, one launch (start us, length us, event | category | flops | bytes accessed | tf_op | source)
XLA Modules:
  0.0 96.1 jit_solution(10934746123491212759)
XLA Ops:
  0.0 0.3 multiply_cosine_fusion
  0.3 0.8 pad_maximum_fusion.table_ref
  1.1 1.6 %copy.15.q_ref = bf16[128,320]{1,0:T(8,128)(2,1)} copy(bf16[128,320]{0,1:T(8,128)(2,1)} %param.11) | data formatting | bytes 163840 | tf_op args[0]
  2.7 1.4 %copy.16.key_ref = bf16[128,64]{1,0:T(8,128)(2,1)} copy(bf16[128,64]{0,1:T(8,128)(2,1)} %param.13) | data formatting | bytes 32768 | tf_op args[2]
  4.2 1.3 %reshape.14.gain_ref = bf16[1,2048]{1,0:T(2,128)(2,1)} reshape(bf16[2048]{0:T(1024)(128)(2,1)} %param.17) | data formatting | bytes 8192 | tf_op jit(solution)/shard_map/reshape | solution.py:522
  5.4 89.1 %shard_map.109 = bf16[32,2048]{1,0:T(8,128)(2,1)} custom-call(f32[128,128]{1,0:T(8,128)} %pad_maximum_fusion.table_ref, bf16[128,320]{1,0:T(8,128)(2,1)} %copy.15.q_ref, bf16[128,512]{1,0:T(8,128)(2,1)} %lat_ref.1, bf16[128,64]{1,0:T(8,128)(2,1)} %copy.16.key_ref, bf16[512,384]{1,0:T(8,128)(2,1)} %expand_ref.1, bf16[128,2048]{1,0:T(8,128)(2,1)} %res_ref.1, ...), custom_call_target="tpu_custom_call" | custom-call | tf_op jit(solution)/shard_map/pallas_call | solution.py:494
  94.5 1.6 %copy.18 = bf16[32,2048]{1,0:T(8,128)(2,1)} copy(bf16[32,2048]{1,0:T(8,128)(2,1)} %shard_map.109) | data formatting | bytes 262144
  (2 shorter events, 0.0 us)

commit v2 on v1

--- a/solution.py
+++ b/solution.py
@@ -200,15 +200,20 @@
     q_ref,
     lat_ref,
     key_ref,
+    conv_ref,
+    expand_hbm,
+    res_hbm,
+    out_w_hbm,
+    gate_hbm,
+    value_hbm,
+    down_hbm,
+    out_ref,
     expand_ref,
     res_ref,
     out_w_ref,
-    gain_ref,
     gate_ref,
     value_ref,
-    conv_ref,
     down_ref,
-    out_ref,
     lat_all,
     att_send,
     att_recv,
@@ -228,6 +233,7 @@
     x_recv,
     z_send,
     z_recv,
+    in_s,
     lz_s, lz_r, ly_s, ly_r, lc_s, lc_r,
     wz_s, wz_r, wy_s, wy_r,
     dz_s, dz_r, dy_s, dy_r,
@@ -241,7 +247,7 @@
     z, y = s // 2, s % 2
     x, c = t // 2, t % 2
     yo, xo, co = 1 - y, 1 - x, 1 - c
-    rows = q_ref.shape[0]
+    rows = lat_ref.shape[0]
     half, share = rows // 2, rows // 4
     rank = lat_ref.shape[1]
     sub = down_ref.shape[0] // zn
@@ -279,16 +285,34 @@
     for dev in partners:
         pl.semaphore_signal(barrier, inc=1, device_id=dev, device_id_type=MESH)
 
-    cos2 = table_ref[:, : 2 * (ROPE // 2)]
-    sin2 = table_ref[:, ROPE : 2 * ROPE]
+    mine_rows = pl.ds(pl.multiple_of(t * share, share), share)
+    loads = [
+        pltpu.make_async_copy(src, dst, in_s.at[i])
+        for i, (src, dst) in enumerate(
+            [
+                (gate_hbm, gate_ref),
+                (value_hbm, value_ref),
+                (down_hbm, down_ref),
+                (expand_hbm, expand_ref),
+                (res_hbm.at[mine_rows, :], res_ref),
+                (out_w_hbm, out_w_ref),
+            ]
+        )
+    ]
+    for load in loads:
+        load.start()
+
+    h = ROPE // 2
+    cos, sine = table_ref[:h, :], table_ref[h:ROPE, :]
 
     def turn(v):
-        v = v.astype(f32)
-        h = ROPE // 2
-        swapped = jnp.concatenate([v[:, h:], v[:, :h]], axis=1)
-        return (v * cos2 + swapped * sin2).astype(bf16)
-
-    key_turned = turn(key_ref[...])
+        a, b = v[:h], v[h:]
+        return jnp.concatenate([a * cos - b * sine, b * cos + a * sine], axis=0)
+
+    rot = NOPE_A + NOPE_B
+    q = q_ref[...].astype(f32)
+    pair = jnp.concatenate([turn(q[rot + ROPE :]), turn(key_ref[...].astype(f32))], axis=0).T.astype(bf16)
+    q_narrow_t, key_turned = pair[:, :ROPE], pair[:, ROPE:]
     for i in range(2):
         lat_all[s, i, :, :rank] = lat_ref[i * half : (i + 1) * half, :]
         lat_all[s, i, :, rank : rank + ROPE] = key_turned[i * half : (i + 1) * half, :]
@@ -300,32 +324,38 @@
         send(mine, mine, lz_s.at[d], lz_r.at[d], to_z(d))
     send(mine, mine, ly_s.at[0], ly_r.at[0], y_dev)
 
+    loads[0].wait()
+    loads[1].wait()
     for k in range(zn):
         stage[k, :, :sub] = gate_ref[:, k * sub : (k + 1) * sub]
         stage[k, :, sub:] = value_ref[:, k * sub : (k + 1) * sub]
+    for d in range(1, zn):
+        send(stage.at[(z + d) % zn], w_full.at[s], wz_s.at[d], wz_r.at[d], to_z(d))
+    w_full[s] = stage[z]
+    loads[2].wait()
+
+    def send_down(d):
+        zz = (z + d) % zn
+        piece = down_ref.at[pl.ds(pl.multiple_of(zz * sub, sub), sub), :]
+        send(piece, dn_full.at[s], dz_s.at[d], dz_r.at[d], to_z(d))
+
+    send_down(1)
+    dn_full[s] = down_ref[pl.ds(pl.multiple_of(z * sub, sub), sub), :]
 
     for d in range(1, zn):
         blk = lat_all.at[2 * from_z(d) + y, c]
         arrived(blk, lz_s.at[d], lz_r.at[d])
         send(blk, blk, ly_s.at[d], ly_r.at[d], y_dev)
         send(blk, blk, lc_s.at[d], lc_r.at[d], c_dev)
-    w_full[s] = stage[z]
-    dn_full[s] = down_ref[pl.ds(pl.multiple_of(z * sub, sub), sub), :]
-    for d in range(1, zn):
-        zz = (z + d) % zn
-        send(stage.at[zz], w_full.at[s], wz_s.at[d], wz_r.at[d], to_z(d))
-        send(down_ref.at[pl.ds(pl.multiple_of(zz * sub, sub), sub), :], dn_full.at[s], dz_s.at[d], dz_r.at[d], to_z(d))
+    send(w_full.at[s], w_full.at[s], wy_s.at[0], wy_r.at[0], y_dev)
     for d in range(zn):
         blk = lat_all.at[2 * from_z(d) + yo, c]
         arrived(blk, ly_s.at[d], ly_r.at[d])
         send(blk, blk, lc_s.at[zn + d], lc_r.at[zn + d], c_dev)
-    send(w_full.at[s], w_full.at[s], wy_s.at[0], wy_r.at[0], y_dev)
-    send(dn_full.at[s], dn_full.at[s], dy_s.at[0], dy_r.at[0], y_dev)
-    q_wide = q_ref[:, :NOPE_A]
-    q_narrow = q_ref[:, NOPE_A : NOPE_A + NOPE_B]
-    rot = NOPE_A + NOPE_B
-    q_wide_t = turn(q_ref[:, rot : rot + ROPE])
-    q_narrow_t = turn(q_ref[:, rot + ROPE : rot + 2 * ROPE])
+    q_wide = q[:NOPE_A].T.astype(bf16)
+    pair = jnp.concatenate([q[NOPE_A:rot], turn(q[rot : rot + ROPE])], axis=0).T.astype(bf16)
+    q_narrow, q_wide_t = pair[:, :NOPE_B], pair[:, NOPE_B:]
+    loads[3].wait()
     for d in range(1, zn):
         arrived(lat_all.at[2 * from_z(d) + y, co], lc_s.at[d], lc_r.at[d])
     for d in range(zn):
@@ -360,14 +390,16 @@
         send(att_send.at[o], att_recv.at[t], at_s.at[i], at_r.at[i], {"sp": s, "tp": o})
     att_recv[t] = att_send[t]
 
+    def forward(full, sz, rz, sy, ry, d):
+        blk = full.at[2 * from_z(d) + y]
+        arrived(blk, sz.at[d], rz.at[d])
+        send(blk, blk, sy.at[d], ry.at[d], y_dev)
+
     def forward_weights(d):
-        blk = w_full.at[2 * from_z(d) + y]
-        arrived(blk, wz_s.at[d], wz_r.at[d])
-        send(blk, blk, wy_s.at[d], wy_r.at[d], y_dev)
-        blk = dn_full.at[2 * from_z(d) + y]
-        arrived(blk, dz_s.at[d], dz_r.at[d])
-        send(blk, blk, dy_s.at[d], dy_r.at[d], y_dev)
-
+        forward(w_full, wz_s, wz_r, wy_s, wy_r, d)
+
+    loads[4].wait()
+    loads[5].wait()
     for i, o in enumerate(others):
         arrived(att_recv.at[o], at_s.at[i], at_r.at[i])
     projected = jnp.dot(att_recv[0, :, :vals], out_w_ref[:vals, :], preferred_element_type=f32)
@@ -375,17 +407,20 @@
         projected += jnp.dot(
             att_recv[i, :, :vals], out_w_ref[i * vals : (i + 1) * vals, :], preferred_element_type=f32
         )
-    mine_rows = pl.ds(pl.multiple_of(t * share, share), share)
-    stream = (res_ref[mine_rows, :].astype(f32) + projected).astype(bf16)
+    stream = (res_ref[...].astype(f32) + projected).astype(bf16)
     stream_f = stream.astype(f32)
     scaled = stream_f * lax.rsqrt(jnp.mean(stream_f * stream_f, axis=1, keepdims=True) + 1e-06)
-    nrm[z, t] = (scaled * gain_ref[...].astype(f32)).astype(bf16)
+    for k in range(scaled.shape[1] // rows):
+        gain = table_ref[ROPE + k : ROPE + k + 1, :]
+        nrm[z, t, :, k * rows : (k + 1) * rows] = (scaled[:, k * rows : (k + 1) * rows] * gain).astype(bf16)
 
     own = nrm.at[z, t]
     for d in range(1, zn):
         send(own, own, nz_s.at[d], nz_r.at[d], to_z(d))
     send(own, own, nx_s.at[0], nx_r.at[0], x_dev)
     send(own, own, nc_s.at[0], nc_r.at[0], c_dev)
+    for d in range(2, zn):
+        send_down(d)
     forward_weights(1)
     xt = 2 * xo + c
     blk = nrm.at[z, xt]
@@ -402,6 +437,8 @@
         blk = nrm.at[from_z(d), xt]
         arrived(blk, nx_s.at[d], nx_r.at[d])
         send(blk, blk, nc_s.at[zn + d], nc_r.at[zn + d], c_dev)
+    send(dn_full.at[s], dn_full.at[s], dy_s.at[0], dy_r.at[0], y_dev)
+    forward(dn_full, dz_s, dz_r, dy_s, dy_r, 1)
     for d in range(zn):
         arrived(w_full.at[2 * from_z(d) + yo], wy_s.at[d], wy_r.at[d])
     weights = w_full[...].reshape(sp * w_full.shape[1], 2 * sub)
@@ -412,6 +449,8 @@
         block = nrm[zz].reshape(rows, nrm.shape[3])
         hbuf[zz] = jnp.dot(block, weights, preferred_element_type=f32).astype(bf16)
 
+    for d in range(2, zn):
+        forward(dn_full, dz_s, dz_r, dy_s, dy_r, d)
     wide_lanes = halo_send.shape[1]
     for k in range(zn):
         g = hbuf[k, :, :wide_lanes].astype(f32)
@@ -482,21 +521,28 @@
     d_own = gate_weight.shape[0]
     positions = lax.axis_index("sp") * rows + jnp.arange(rows, dtype=jnp.int32)
     cos_table, sine_table = tables(positions, ROPE)
-    table = jnp.concatenate([cos_table, cos_table, -sine_table, sine_table], axis=1)
+    gain = norm_gain.reshape(width // rows, rows).astype(jnp.float32)
+    table = jnp.concatenate([cos_table.T, sine_table.T, gain], axis=0)
     bf16, f32 = jnp.bfloat16, jnp.float32
     vals = VAL_A + VAL_B
     lanes = -(-vals // 128) * 128
     halo_lanes = -(-sub // 128) * 128
     V, DMA = pltpu.VMEM, pltpu.SemaphoreType.DMA
-    sems = []
+    sems = [DMA((6,))]
     for count in (zn, zn, 2 * zn, zn, zn, zn, zn, 3, zn, zn, 2 * zn, 1, zn, zn, zn):
         sems += [DMA((count,)), DMA((count,))]
     return pl.pallas_call(
         functools.partial(layer_kernel, zn),
         out_shape=jax.ShapeDtypeStruct((share, width), bf16),
-        in_specs=[pl.BlockSpec(memory_space=V)] * 12,
+        in_specs=[pl.BlockSpec(memory_space=V)] * 5 + [pl.BlockSpec(memory_space=pl.ANY)] * 6,
         out_specs=pl.BlockSpec(memory_space=V),
         scratch_shapes=[
+            V(expand_weight.shape, bf16),
+            V((share, width), bf16),
+            V(out_weight.shape, bf16),
+            V(gate_weight.shape, bf16),
+            V(value_weight.shape, bf16),
+            V(down_weight.shape, bf16),
             V((2 * zn, 2, half, latents.shape[1] + 2 * ROPE), bf16),
             V((4, share, lanes), bf16),
             V((4, share, lanes), bf16),
@@ -518,8 +564,8 @@
             V((zn, share, width), bf16),
         ] + sems,
         compiler_params=pltpu.CompilerParams(collective_id=0, has_side_effects=True),
-    )(table, queries, latents, shared_key, expand_weight, residual, out_weight,
-      norm_gain.reshape(1, -1), gate_weight, value_weight, conv_weight, down_weight)
+    )(table, queries.T, latents, shared_key.T, conv_weight, expand_weight, residual, out_weight,
+      gate_weight, value_weight, down_weight)
 
 
 def pick(*args):
@@ -532,7 +578,8 @@
         and hidden % zn == 0
         and sub % 64 == 0
         and args[7].shape[0] % 128 == 0
-        and args[0].shape[0] % 64 == 0
+        and args[0].shape[0] % 128 == 0
+        and args[4].shape[1] % args[0].shape[0] == 0
         and args[9].shape[0] == 3
     )
     return kernel_body(zn, *args) if fits else body(*args)

time: 97.2 us -> 91.9 us (0.945)
  local copies, waits for them, and re-layouts: 5.91 us -> 1.57 us
    unnamed x3 -> x1, local copies, waits for them, and re-layouts: 4.63 us -> 1.57 us
    reshape x1 -> x0, local copies, waits for them, and re-layouts: 1.28 us -> none  [kernel_body(): norm_gain.reshape(1, -1)]
where the time goes in v2:
time: 91.9 us; the launch traced here: 91.7 us
  Pallas kernels  88.6 us (96%)
  local copies, waits for them, and re-layouts  1.57 us (2%)
  other arithmetic  1.47 us (2%)
    pallas_call x1, Pallas kernels, kernel_body(): pl.pallas_call(functools.partial(layer_kernel, zn), out_shape=jax.ShapeDt...  88.6 us

profile of v2, /device:TPU:0, one launch (start us, length us, event | category | flops | bytes accessed | tf_op | source)
XLA Modules:
  0.0 91.7 jit_solution(9149495733756896921)
XLA Ops:
  0.0 0.7 bitcast_convert_fusion
  0.7 0.1 multiply_cosine_fusion
  0.9 0.6 pad_maximum_fusion.table_ref
  1.5 88.6 %shard_map.109 = bf16[32,2048]{1,0:T(8,128)(2,1)} custom-call(f32[80,128]{1,0:T(8,128)} %pad_maximum_fusion.table_ref, bf16[320,128]{1,0:T(8,128)(2,1)} %bitcast.5, bf16[128,512]{1,0:T(8,128)(2,1)} %lat_ref.1, bf16[64,128]{1,0:T(8,128)(2,1)} %bitcast.6, bf16[3,768]{1,0:T(4,128)(2,1)} %conv_ref.1, bf16[512,384]{1,0:T(8,128)(2,1)} %expand_hbm.1, ...), custom_call_target="tpu_custom_call" | custom-call | tf_op jit(solution)/shard_map/pallas_call | solution.py:534
  90.1 1.6 %copy.13 = bf16[32,2048]{1,0:T(8,128)(2,1)} copy(bf16[32,2048]{1,0:T(8,128)(2,1)} %shard_map.109) | data formatting | bytes 262144
  (2 shorter events, 0.0 us)

commit v3 on v2

--- a/solution.py
+++ b/solution.py
@@ -449,14 +449,14 @@
         block = nrm[zz].reshape(rows, nrm.shape[3])
         hbuf[zz] = jnp.dot(block, weights, preferred_element_type=f32).astype(bf16)
 
-    for d in range(2, zn):
-        forward(dn_full, dz_s, dz_r, dy_s, dy_r, d)
     wide_lanes = halo_send.shape[1]
     for k in range(zn):
         g = hbuf[k, :, :wide_lanes].astype(f32)
         halo_send[k : k + 1, :] = g[rows - 1 : rows, :]
         halo_send[zn + k : zn + k + 1, :] = g[0:1, :]
     send(halo_send, halo_recv, h_s.at[0], h_r.at[0], y_dev)
+    for d in range(2, zn):
+        forward(dn_full, dz_s, dz_r, dy_s, dy_r, d)
     taps = jnp.zeros((conv_ref.shape[0], wide_lanes), f32)
     conv_all = conv_ref[...].astype(f32)
     pieces = [conv_all[:, k * sub : (k + 1) * sub] for k in range(zn)]

time: 91.9 us -> 91.4 us (level)
  no operation moved by 1% of the time
where the time goes in v3:
time: 91.4 us; the launch traced here: 91.3 us
  Pallas kernels  88.2 us (96%)
  local copies, waits for them, and re-layouts  1.57 us (2%)
  other arithmetic  1.47 us (2%)
    pallas_call x1, Pallas kernels, kernel_body(): pl.pallas_call(functools.partial(layer_kernel, zn), out_shape=jax.ShapeDt...  88.2 us

profile of v3, /device:TPU:0, one launch (start us, length us, event | category | flops | bytes accessed | tf_op | source)
XLA Modules:
  0.0 91.3 jit_solution(4614274909899172051)
XLA Ops:
  0.0 0.7 bitcast_convert_fusion
  0.7 0.1 multiply_cosine_fusion
  0.9 0.6 pad_maximum_fusion.table_ref
  1.5 88.2 %shard_map.109 = bf16[32,2048]{1,0:T(8,128)(2,1)} custom-call(f32[80,128]{1,0:T(8,128)} %pad_maximum_fusion.table_ref, bf16[320,128]{1,0:T(8,128)(2,1)} %bitcast.5, bf16[128,512]{1,0:T(8,128)(2,1)} %lat_ref.1, bf16[64,128]{1,0:T(8,128)(2,1)} %bitcast.6, bf16[3,768]{1,0:T(4,128)(2,1)} %conv_ref.1, bf16[512,384]{1,0:T(8,128)(2,1)} %expand_hbm.1, ...), custom_call_target="tpu_custom_call" | custom-call | tf_op jit(solution)/shard_map/pallas_call | solution.py:534
  89.7 1.6 %copy.13 = bf16[32,2048]{1,0:T(8,128)(2,1)} copy(bf16[32,2048]{1,0:T(8,128)(2,1)} %shard_map.109) | data formatting | bytes 262144
  (2 shorter events, 0.0 us)
